TPU v7x, 32 devices: a whole 2x2x4 slice. The times are simulated.
32 devices in a mesh: sp: 4 (over z), tp: 4 (over y, x), dp: 2 (over core).
Axes of the slice: x: 2, y: 2, z: 4, core: 2. Of those that a mesh axis runs over, the one named last changes fastest.
Arguments:
- latent_in: bfloat16 [3072, 2048], P(('dp', 'sp', 'tp')), parts along dimension 0, may hold values from -6 to 6
- condition: bfloat16 [4096], P(('dp', 'sp')), parts along dimension 0, may hold values from -8 to 8
- context_latent: bfloat16 [1024, 256], P(('dp', 'sp')), parts along dimension 0, may hold values from -6 to 6
- context_rope: bfloat16 [1024, 64], P(('dp', 'sp')), parts along dimension 0, may hold values from -6 to 6
- shift_weight: bfloat16 [2048, 2048], P('sp', 'tp'), may hold values from -0.125 to 0.125
- scale_weight: bfloat16 [2048, 2048], P('sp', 'tp'), may hold values from -0.125 to 0.125
- gate_weight: bfloat16 [2048, 2048], P('sp', 'tp'), may hold values from -0.125 to 0.125
- norm_gain: float32 [2048], replicated, may hold values from 0.1 to 1.9
- down_query: bfloat16 [2048, 512], replicated, may hold values from -0.125 to 0.125
- down_latent: bfloat16 [2048, 256], replicated, may hold values from -0.125 to 0.125
- down_rope: bfloat16 [2048, 64], replicated, may hold values from -0.125 to 0.125
- query_gain: float32 [512], replicated, may hold values from 0.5 to 60
- latent_gain: float32 [256], replicated, may hold values from 0.1 to 1.9
- up_query: bfloat16 [512, 1536], P(None, 'tp'), may hold values from -0.25 to 0.25
- up_key: bfloat16 [256, 1024], P(None, 'tp'), may hold values from -0.375 to 0.375
- up_value: bfloat16 [256, 1024], P(None, 'tp'), may hold values from -0.375 to 0.375
- context_bias: float32 [8], P('tp'), may hold values from 1 to 2.5
- out_weight: bfloat16 [1024, 2048], replicated, may hold values from -3 to 3
Outputs:
- mixed_out: bfloat16 [3072, 2048], P(('dp', 'sp', 'tp')), parts along dimension 0
There are 2 independent parts, one for each index of `dp`. A program takes and returns all parts, laid end to end along the dimension named above; an argument that names none is the same for every part. Nothing has to cross between parts.
All inputs are finite; a program needn't handle non-finite values.
Results may differ from a plain program's by a relative error of at most 0.039.
The roundings to bfloat16 on the way count: a program that leaves them out, or rounds other values in their place, can miss the bound.
Values may be sent and summed in bfloat16 or wider, within the bound.
A program may use at most 128 MiB of HBM per device.

v0:
```python
import jax
import jax.numpy as jnp
from jax import lax
from jax.sharding import PartitionSpec as P

QK_NOPE = 128
QK_ROPE = 64
V_HEAD = 128
GRID_W = 64
epsilon = 1e-06
rope_base = 10000.0
block_limit = 2048


def rms_scaled(values, gain_vec):
    mean_sq = jnp.mean(values * values, axis=-1, keepdims=True)
    return values * lax.rsqrt(mean_sq + epsilon) * gain_vec


def rope_tables(positions, rope_width):
    freq_count = rope_width // 4
    inverse = rope_base ** (-jnp.arange(freq_count, dtype=jnp.float32) / freq_count)
    grid_row = (positions // GRID_W).astype(jnp.float32)
    grid_col = (positions % GRID_W).astype(jnp.float32)
    row_angle = grid_row[:, None] * inverse
    col_angle = grid_col[:, None] * inverse
    angles = jnp.concatenate([row_angle, row_angle, col_angle, col_angle], axis=-1)
    return (jnp.cos(angles), jnp.sin(angles))


def rope_turn(values, cosine_table, sine_table):
    part_one, part_two, part_three, part_four = jnp.split(values, 4, axis=-1)
    turned = jnp.concatenate([-part_two, part_one, -part_four, part_three], axis=-1)
    return values * cosine_table + turned * sine_table


def attend(attn_state, query_nope, query_rope, keys_nope, values_in, keys_rope, bias_col):
    score_scale = (query_nope.shape[-1] + query_rope.shape[-1]) ** (-0.5)
    scores = jnp.einsum("thd,khd->htk", query_nope, keys_nope, preferred_element_type=jnp.float32)
    scores = scores + jnp.einsum(
        "thr,kr->htk", query_rope, keys_rope, preferred_element_type=jnp.float32
    )
    scores = scores * score_scale + bias_col
    run_max, run_total, run_acc = attn_state
    new_max = jnp.maximum(run_max, jnp.max(scores, axis=-1))
    shrink = jnp.exp(run_max - new_max)
    weights = jnp.exp(scores - new_max[:, :, None])
    new_total = run_total * shrink + jnp.sum(weights, axis=-1)
    new_acc = run_acc * shrink[:, :, None] + jnp.einsum(
        "htk,khd->htd", weights.astype(jnp.bfloat16), values_in, preferred_element_type=jnp.float32
    )
    return (new_max, new_total, new_acc)


def over_blocks(attn_state, arrays, handle):
    row_count = arrays[0].shape[0]
    block_rows = 1
    for candidate in range(min(row_count, block_limit), 0, -1):
        if row_count % candidate == 0:
            block_rows = candidate
            break
    block_count = row_count // block_rows
    if block_count == 1:
        return handle(attn_state, arrays)
    stacked = tuple(
        (array_in.reshape((block_count, block_rows) + array_in.shape[1:]) for array_in in arrays)
    )

    def one_turn(inner_state, pieces):
        return (handle(inner_state, pieces), None)

    return lax.scan(one_turn, attn_state, stacked)[0]


def on_device(
    latent_in,
    condition,
    context_latent,
    context_rope,
    shift_weight,
    scale_weight,
    gate_weight,
    norm_gain,
    down_query,
    down_latent,
    down_rope,
    query_gain,
    latent_gain,
    up_query,
    up_key,
    up_value,
    context_bias,
    out_weight,
):
    activated = jax.nn.silu(condition.astype(jnp.float32)).astype(jnp.bfloat16)
    partials = jnp.stack(
        [
            jnp.dot(activated, weight_in, preferred_element_type=jnp.float32)
            for weight_in in (shift_weight, scale_weight, gate_weight)
        ]
    )
    summed = lax.psum(partials, "sp")
    modulation = lax.all_gather(summed, "tp", axis=1, tiled=True)
    shift_vec = modulation[0]
    scale_vec = modulation[1]
    gate_vec = modulation[2]
    residual_in = latent_in.astype(jnp.float32)
    normed = (rms_scaled(residual_in, norm_gain) * (1.0 + scale_vec) + shift_vec).astype(
        jnp.bfloat16
    )
    query_low = rms_scaled(
        jnp.dot(normed, down_query, preferred_element_type=jnp.float32), query_gain
    ).astype(jnp.bfloat16)
    latent_low = rms_scaled(
        jnp.dot(normed, down_latent, preferred_element_type=jnp.float32), latent_gain
    ).astype(jnp.bfloat16)
    local_rows = latent_in.shape[0]
    first_row = (lax.axis_index("sp") * lax.axis_size("tp") + lax.axis_index("tp")) * local_rows
    own_positions = first_row + jnp.arange(local_rows, dtype=jnp.int32)
    own_cosine, own_sine = rope_tables(own_positions, QK_ROPE)
    rope_keys = rope_turn(
        jnp.dot(normed, down_rope, preferred_element_type=jnp.float32), own_cosine, own_sine
    ).astype(jnp.bfloat16)
    query_group, latent_group, rope_group = (
        lax.all_gather(query_low, "tp", axis=0, tiled=True),
        lax.all_gather(latent_low, "tp", axis=0, tiled=True),
        lax.all_gather(rope_keys, "tp", axis=0, tiled=True),
    )
    group_rows = query_group.shape[0]
    group_positions = lax.axis_index("sp") * group_rows + jnp.arange(group_rows, dtype=jnp.int32)
    group_cosine, group_sine = rope_tables(group_positions, QK_ROPE)
    head_count = up_key.shape[1] // QK_NOPE
    queries = jnp.dot(query_group, up_query, preferred_element_type=jnp.float32).reshape(
        group_rows, head_count, QK_NOPE + QK_ROPE
    )
    query_nope = queries[:, :, :QK_NOPE].astype(jnp.bfloat16)
    query_rope = rope_turn(
        queries[:, :, QK_NOPE:], group_cosine[:, None, :], group_sine[:, None, :]
    ).astype(jnp.bfloat16)
    context_all, context_keys_rope = (
        lax.all_gather(context_latent, "sp", axis=0, tiled=True),
        lax.all_gather(context_rope, "sp", axis=0, tiled=True),
    )
    context_count = context_all.shape[0]
    context_nope = (
        jnp.dot(context_all, up_key, preferred_element_type=jnp.float32)
        .astype(jnp.bfloat16)
        .reshape(context_count, head_count, QK_NOPE)
    )
    context_values = (
        jnp.dot(context_all, up_value, preferred_element_type=jnp.float32)
        .astype(jnp.bfloat16)
        .reshape(context_count, head_count, V_HEAD)
    )
    start_state = (
        jnp.full((head_count, group_rows), -jnp.inf, jnp.float32),
        jnp.zeros((head_count, group_rows), jnp.float32),
        jnp.zeros((head_count, group_rows, V_HEAD), jnp.float32),
    )
    bias_col = context_bias[:, None, None]

    def context_step(inner_state, pieces):
        return attend(
            inner_state, query_nope, query_rope, pieces[0], pieces[1], pieces[2], bias_col
        )

    attn_state = over_blocks(
        start_state, (context_nope, context_values, context_keys_rope), context_step
    )
    own_nope = jnp.dot(latent_group, up_key, preferred_element_type=jnp.float32).astype(
        jnp.bfloat16
    )
    own_values = jnp.dot(latent_group, up_value, preferred_element_type=jnp.float32).astype(
        jnp.bfloat16
    )

    def expanded_step(inner_state, pieces):
        piece_rows = pieces[0].shape[0]
        return attend(
            inner_state,
            query_nope,
            query_rope,
            pieces[0].reshape(piece_rows, head_count, QK_NOPE),
            pieces[1].reshape(piece_rows, head_count, V_HEAD),
            pieces[2],
            0.0,
        )

    attn_state = over_blocks(
        attn_state,
        (
            lax.all_gather(own_nope, "sp", axis=0, tiled=True),
            lax.all_gather(own_values, "sp", axis=0, tiled=True),
            lax.all_gather(rope_group, "sp", axis=0, tiled=True),
        ),
        expanded_step,
    )
    attended = (attn_state[2] / attn_state[1][:, :, None]).astype(jnp.bfloat16)
    attended = attended.transpose(1, 0, 2).reshape(group_rows, head_count * V_HEAD)
    token_major = lax.all_to_all(attended, "tp", split_axis=0, concat_axis=1, tiled=True)
    mixed = jnp.dot(token_major, out_weight, preferred_element_type=jnp.float32)
    return (residual_in + gate_vec * mixed).astype(jnp.bfloat16)


def solution(mesh):
    in_specs = (
        P(("dp", "sp", "tp"), None),
        P(("dp", "sp")),
        P(("dp", "sp"), None),
        P(("dp", "sp"), None),
        P("sp", "tp"),
        P("sp", "tp"),
        P("sp", "tp"),
        P(),
        P(),
        P(),
        P(),
        P(),
        P(),
        P(None, "tp"),
        P(None, "tp"),
        P(None, "tp"),
        P("tp"),
        P(),
    )
    out_specs = P(("dp", "sp", "tp"), None)
    return jax.shard_map(
        on_device, mesh=mesh, in_specs=in_specs, out_specs=out_specs, check_vma=False
    )
```

profile of v0, /device:TPU:0, one launch (start us, length us, event | category | flops | bytes accessed | tf_op | source)
XLA Modules:
  0.0 158.6 jit_solution(2897633564219635338)
XLA Ops:
  0.6 0.7 fusion.54
  1.3 1.2 fusion.72
  2.6 1.2 fusion.73
  3.8 1.3 fusion.74
  5.1 13.8 %psum.7 = f32[3,512]{1,0:T(4,128)S(1)} all-reduce(f32[3,512]{1,0:T(4,128)S(1)} %pad_maximum_fusion.2), channel_id=1, replica_groups=mesh['sp'=4,'tp'=4,'dp'=2] {'sp'}, use_global_device_ids=true, to_apply=%region_0.1 | all-reduce | flops 1536 | bytes 12288 | tf_op jit(solution)/shard_map/psum | solution.py:102
  18.9 8.2 %all_gather.27 = f32[3,2048]{1,0:T(4,128)S(1)} all-gather(f32[3,512]{1,0:T(4,128)S(1)} %psum.7), channel_id=1, replica_groups=mesh['sp'=4,'tp'=4,'dp'=2] {'tp'}, dimensions={1}, use_global_device_ids=true | all-gather | bytes 30720 | tf_op jit(solution)/shard_map/all_gather | solution.py:103
  27.1 1.2 fusion.26
  28.4 1.9 %multiply_reduce_fusion.1 = (f32[96]{0:T(128)S(1)}, f32[96,256]{1,0:T(8,128)S(1)}) fusion(bf16[2048,256]{1,0:T(8,128)(2,1)} %param.27, bf16[96,2048]{1,0:T(8,128)(2,1)} %param.18, f32[2048]{0:T(1024)S(1)} %bitcast.119, f32[2048]{0:T(1024)S(1)} %bitcast.122, f32[2048]{0:T(1024)} %param.25, f32[96]{0:T(128)S(1)} %add_rsqrt_fusion.2), kind=kOutput, calls=%fused_computation.50 | convolution fusion | flops 101892000 | bytes 1565440 | tf_op jit(solution)/shard_map/dot_general | solution.py:115
  30.3 8.7 %all_gather.31 = bf16[384,256]{1,0:T(8,128)(2,1)S(1)} all-gather(bf16[96,256]{1,0:T(8,128)(2,1)S(1)} %multiply_convert_fusion.1), channel_id=1, replica_groups=mesh['sp'=4,'tp'=4,'dp'=2] {'tp'}, dimensions={0}, use_global_device_ids=true | all-gather | bytes 245760 | tf_op jit(solution)/shard_map/all_gather | solution.py:126
  39.1 13.8 %all_gather.29 = bf16[512,256]{1,0:T(8,128)(2,1)S(1)} all-gather(bf16[128,256]{1,0:T(8,128)(2,1)S(1)} %copy-done.12), channel_id=1, replica_groups=mesh['sp'=4,'tp'=4,'dp'=2] {'sp'}, dimensions={0}, use_global_device_ids=true | all-gather | bytes 327680 | tf_op jit(solution)/shard_map/all_gather | solution.py:141
  52.9 0.9 convolution_convert_fusion.3
  54.0 1.0 convolution_convert_fusion
  56.0 8.5 %all_gather.28 = bf16[384,512]{1,0:T(8,128)(2,1)S(1)} all-gather(bf16[96,512]{1,0:T(8,128)(2,1)S(1)} %multiply_convert_fusion), channel_id=1, replica_groups=mesh['sp'=4,'tp'=4,'dp'=2] {'tp'}, dimensions={0}, use_global_device_ids=true | all-gather | bytes 491520 | tf_op jit(solution)/shard_map/all_gather | solution.py:125
  65.0 0.7 slice_negate_fusion.1
  66.3 1.3 fusion.62
  67.6 0.6 copy-done.11
  68.9 0.7 broadcast_multiply_fusion.3
  69.6 0.9 fusion.47
  70.5 8.2 %all-gather = bf16[4,96,64]{1,2,0:T(8,128)(2,1)S(1)} all-gather(bf16[1,96,64]{1,2,0:T(8,128)(2,1)S(1)} %fusion.47), channel_id=1, replica_groups=mesh['sp'=4,'tp'=4,'dp'=2] {'tp'}, dimensions={0}, use_global_device_ids=true | all-gather | bytes 61440 | tf_op jit(solution)/shard_map/all_gather | solution.py:127
  78.7 0.7 copy.48
  79.4 1.6 reshape.254
  81.0 14.6 %all_gather.34 = bf16[1536,64]{0,1:T(8,128)(2,1)S(1)} all-gather(bf16[384,64]{0,1:T(8,128)(2,1)} %reshape.254), channel_id=1, replica_groups=mesh['sp'=4,'tp'=4,'dp'=2] {'sp'}, dimensions={0}, use_global_device_ids=true | all-gather | bytes 245760 | tf_op jit(solution)/shard_map/all_gather | solution.py:194
  95.6 16.9 %all_gather.32 = bf16[1536,256]{1,0:T(8,128)(2,1)S(1)} all-gather(bf16[384,256]{1,0:T(8,128)(2,1)} %convolution_convert_fusion.3), channel_id=1, replica_groups=mesh['sp'=4,'tp'=4,'dp'=2] {'sp'}, dimensions={0}, use_global_device_ids=true | all-gather | bytes 983040 | tf_op jit(solution)/shard_map/all_gather | solution.py:192
  112.9 12.2 %all_gather.30 = bf16[512,64]{0,1:T(8,128)(2,1)S(1)} all-gather(bf16[128,64]{0,1:T(8,128)(2,1)S(1)} %copy-done.13), channel_id=1, replica_groups=mesh['sp'=4,'tp'=4,'dp'=2] {'sp'}, dimensions={0}, use_global_device_ids=true | all-gather | bytes 81920 | tf_op jit(solution)/shard_map/all_gather | solution.py:142
  125.4 0.8 fusion.39
  126.3 1.0 fusion.71
  128.3 15.6 %all_gather.35 = bf16[1536,256]{1,0:T(8,128)(2,1)S(1)} all-gather(bf16[384,256]{1,0:T(8,128)(2,1)S(1)} %convolution_convert_fusion.2), channel_id=1, replica_groups=mesh['sp'=4,'tp'=4,'dp'=2] {'sp'}, dimensions={0}, use_global_device_ids=true | all-gather | bytes 983040 | tf_op jit(solution)/shard_map/all_gather | solution.py:193
  143.8 0.8 fusion.1
  144.8 0.7 fusion.19
  145.5 0.9 fusion.23
  146.8 8.1 %all_to_all.19 = bf16[4,96,256]{2,1,0:T(8,128)(2,1)S(1)} all-to-all(bf16[4,96,256]{2,1,0:T(8,128)(2,1)S(1)} %all_to_all.14), channel_id=1, replica_groups=mesh['sp'=4,'tp'=4,'dp'=2] {'tp'}, dimensions={0} | all-to-all | bytes 393216 | tf_op jit(solution)/shard_map/all_to_all | solution.py:200
  154.9 3.8 %fusion.7 = bf16[96,2048]{1,0:T(8,128)(2,1)} fusion(bf16[96,1024]{1,0:T(8,128)(2,1)S(1)} %bitcast.116, bf16[1024,2048]{1,0:T(8,128)(2,1)} %param.35, bf16[96,2048]{1,0:T(8,128)(2,1)S(1)} %copy-done.1, f32[2048]{0:T(1024)S(1)} %bitcast.118), kind=kOutput, calls=%fused_computation.9 | convolution fusion | flops 403439616 | bytes 5185536 | tf_op jit(solution)/shard_map/dot_general | solution.py:201
  (72 shorter events, 5.8 us)
Async XLA Ops:
  0.0 55.3 %copy-start = (bf16[2048,512]{1,0:T(8,128)(2,1)S(1)}, bf16[2048,512]{1,0:T(8,128)(2,1)}, u32[]{:S(2)}) copy-start(bf16[2048,512]{1,0:T(8,128)(2,1)} %param.26) | copy-start | bytes 6291460
  0.0 30.2 %copy-start.19 = (f32[256]{0:T(256)S(1)}, f32[256]{0:T(256)}, u32[]{:S(2)}) copy-start(f32[256]{0:T(256)} %param.30) | copy-start | bytes 3076
  0.0 39.0 %copy-start.12 = (bf16[128,256]{1,0:T(8,128)(2,1)S(1)}, bf16[128,256]{1,0:T(8,128)(2,1)}, u32[]{:S(2)}) copy-start(bf16[128,256]{1,0:T(8,128)(2,1)} %param.20) | copy-start | bytes 196612
  1.3 51.5 %copy-start.3 = (bf16[256,256]{1,0:T(8,128)(2,1)S(1)}, bf16[256,256]{1,0:T(8,128)(2,1)}, u32[]{:S(2)}) copy-start(bf16[256,256]{1,0:T(8,128)(2,1)} %param.32) | copy-start | bytes 393220
  3.8 50.2 %copy-start.4 = (bf16[256,256]{1,0:T(8,128)(2,1)S(1)}, bf16[256,256]{1,0:T(8,128)(2,1)}, u32[]{:S(2)}) copy-start(bf16[256,256]{1,0:T(8,128)(2,1)} %param.33) | copy-start | bytes 393220
  27.1 28.1 %copy-start.14 = (f32[1,2048]{1,0:T(1,128)}, f32[1,2048]{1,0:T(1,128)S(1)}, u32[]{:S(2)}) copy-start(f32[1,2048]{1,0:T(1,128)S(1)} %get-tuple-element.15) | copy-start | bytes 24580
  27.1 27.9 %copy-start.5 = (bf16[256,256]{1,0:T(8,128)(2,1)S(1)}, bf16[256,256]{1,0:T(8,128)(2,1)}, u32[]{:S(2)}) copy-start(bf16[256,256]{1,0:T(8,128)(2,1)} %param.33) | copy-start | bytes 393220
  28.3 26.9 %copy-start.22 = (f32[96]{0:T(128)}, f32[96]{0:T(128)S(1)}, u32[]{:S(2)}) copy-start(f32[96]{0:T(128)S(1)} %add_rsqrt_fusion.2) | copy-start | bytes 1156
  28.3 26.9 %copy-start.1 = (bf16[96,2048]{1,0:T(8,128)(2,1)S(1)}, bf16[96,2048]{1,0:T(8,128)(2,1)}, u32[]{:S(2)}) copy-start(bf16[96,2048]{1,0:T(8,128)(2,1)} %param.18) | copy-start | bytes 1179652
  28.4 26.9 %copy-start.21 = (f32[2048]{0:T(1024)S(1)}, f32[2048]{0:T(1024)}, u32[]{:S(2)}) copy-start(f32[2048]{0:T(1024)} %param.25) | copy-start | bytes 24580
  53.7 2.2 %copy-start.17 = (f32[512]{0:T(512)S(1)}, f32[512]{0:T(512)}, u32[]{:S(2)}) copy-start(f32[512]{0:T(512)} %param.29) | copy-start | bytes 6148
  54.0 10.5 %copy-start.6 = (bf16[512,384]{1,0:T(8,128)(2,1)S(1)}, bf16[512,384]{1,0:T(8,128)(2,1)}, u32[]{:S(2)}) copy-start(bf16[512,384]{1,0:T(8,128)(2,1)} %param.31) | copy-start | bytes 1179652
  67.6 0.6 copy-start.11
  70.5 54.6 %copy-start.15 = (f32[384]{0:T(512)S(1)}, f32[384]{0:T(512)}, u32[]{:S(2)}) copy-start(f32[384]{0:T(512)} %get-tuple-element.33) | copy-start | bytes 4612
  70.5 54.6 %copy-start.16 = (f32[384]{0:T(512)S(1)}, f32[384]{0:T(512)}, u32[]{:S(2)}) copy-start(f32[384]{0:T(512)} %get-tuple-element.34) | copy-start | bytes 4612
  81.0 31.9 %copy-start.13 = (bf16[128,64]{0,1:T(8,128)(2,1)S(1)}, bf16[128,64]{0,1:T(8,128)(2,1)}, u32[]{:S(2)}) copy-start(bf16[128,64]{0,1:T(8,128)(2,1)} %param.21) | copy-start | bytes 49156
  81.0 44.1 %copy-start.18 = (f32[16]{0:T(128)S(1)}, f32[16]{0:T(128)}, u32[]{:S(2)}) copy-start(f32[16]{0:T(128)} %multiply_power_fusion) | copy-start | bytes 196
  81.0 44.4 %copy-start.7 = (f32[384,2,16]{0,2,1:T(8,128)S(1)}, f32[384,2,16]{0,2,1:T(8,128)}, u32[]{:S(2)}) copy-start(f32[384,2,16]{0,2,1:T(8,128)} %get-tuple-element.7) | copy-start | bytes 147460
  81.0 44.4 %copy-start.8 = (f32[384,2,16]{0,2,1:T(8,128)S(1)}, f32[384,2,16]{0,2,1:T(8,128)}, u32[]{:S(2)}) copy-start(f32[384,2,16]{0,2,1:T(8,128)} %get-tuple-element.8) | copy-start | bytes 147460
  81.0 44.4 %copy-start.9 = (f32[384,2,16]{0,2,1:T(8,128)S(1)}, f32[384,2,16]{0,2,1:T(8,128)}, u32[]{:S(2)}) copy-start(f32[384,2,16]{0,2,1:T(8,128)} %get-tuple-element.9) | copy-start | bytes 147460
  81.0 44.4 %copy-start.10 = (f32[384,2,16]{0,2,1:T(8,128)S(1)}, f32[384,2,16]{0,2,1:T(8,128)}, u32[]{:S(2)}) copy-start(f32[384,2,16]{0,2,1:T(8,128)} %get-tuple-element.10) | copy-start | bytes 147460
  126.3 1.0 copy-start.20
  143.8 1.0 copy-start.2
where the time goes:
time: 159 us
  blocking collectives  129 us (81%)
  matrix products  18.4 us (12%)
  other arithmetic  7.9 us (5%)
  local copies, waits for them, and re-layouts  3.43 us (2%)
    all_gather x1, blocking collectives, on_device(): lax.all_gather(own_nope, 'sp', axis=0, tiled=True)  16.9 us
    all_gather x1, blocking collectives, on_device(): lax.all_gather(own_values, 'sp', axis=0, tiled=True)  15.6 us
    all_gather x1, blocking collectives, on_device(): lax.all_gather(rope_group, 'sp', axis=0, tiled=True)  14.6 us
    all_gather x1, blocking collectives, on_device(): lax.all_gather(context_latent, 'sp', axis=0, tiled=True)  13.8 us
    psum x1, blocking collectives, on_device(): summed = lax.psum(partials, 'sp')  13.8 us
    all_gather x1, blocking collectives, on_device(): lax.all_gather(context_rope, 'sp', axis=0, tiled=True)  12.2 us
    all_gather x1, blocking collectives, on_device(): lax.all_gather(latent_low, 'tp', axis=0, tiled=True)  8.7 us
    all_gather x1, blocking collectives, on_device(): lax.all_gather(query_low, 'tp', axis=0, tiled=True)  8.53 us

commit v1 on v0

--- a/solution.py
+++ b/solution.py
@@ -100,7 +100,12 @@
         ]
     )
     summed = lax.psum(partials, "sp")
-    modulation = lax.all_gather(summed, "tp", axis=1, tiled=True)
+    ring = [summed]
+    for hop in range(3):
+        ring.append(lax.ppermute(ring[-1], "tp", [(dev, (dev + 1) % 4) for dev in range(4)]))
+    modulation = jnp.roll(
+        jnp.concatenate(ring[::-1], axis=1), (lax.axis_index("tp") + 1) * ring[0].shape[1], axis=1
+    )
     shift_vec = modulation[0]
     scale_vec = modulation[1]
     gate_vec = modulation[2]

time: 159 us -> 153 us (0.962)
  blocking collectives: 129 us -> 123 us
  starting transfers between devices: 0 us -> 3.68 us
  local copies, waits for them, and re-layouts: 3.43 us -> 0.67 us
  other arithmetic: 7.9 us -> 5.41 us
  waiting for transfers between devices: 0 us -> 2.21 us
    all_gather x1 -> x0, blocking collectives: 8.2 us -> none  [on_device(): modulation = lax.all_gather(summed, 'tp', axis=1, tiled=True)]
    ppermute x0 -> x3, starting transfers between devices: none -> 3.68 us  [on_device(): lax.ppermute(ring[-1], 'tp', [(dev, (dev + 1) % 4) for dev in range(4)])]
    ppermute x0 -> x3, waiting for transfers between devices: none -> 2.21 us  [on_device(): lax.ppermute(ring[-1], 'tp', [(dev, (dev + 1) % 4) for dev in range(4)])]
    unnamed x47 -> x44, local copies, waits for them, and re-layouts: 2.39 us -> 0.25 us
  transfers between devices with their start and end apart: 0 -> 3, of which waited for: 0 -> 1; matrix products, arithmetic and copies ran while one was open for 0% -> 2% of each run, Pallas kernels for 0% -> 0%
where the time goes in v1:
time: 153 us; the launch traced here: 152 us
  blocking collectives  123 us (80%)
  matrix products  17.3 us (11%)
  other arithmetic  5.41 us (4%)
  starting transfers between devices  3.68 us (2%)
  waiting for transfers between devices  2.21 us (1%)
    all_gather x1, blocking collectives, on_device(): lax.all_gather(own_nope, 'sp', axis=0, tiled=True)  17.7 us
    all_gather x1, blocking collectives, on_device(): lax.all_gather(own_values, 'sp', axis=0, tiled=True)  15.6 us
    all_gather x1, blocking collectives, on_device(): lax.all_gather(rope_group, 'sp', axis=0, tiled=True)  14.1 us
    all_gather x1, blocking collectives, on_device(): lax.all_gather(context_latent, 'sp', axis=0, tiled=True)  14.1 us
    psum x1, blocking collectives, on_device(): summed = lax.psum(partials, 'sp')  13.7 us
    all_gather x1, blocking collectives, on_device(): lax.all_gather(context_rope, 'sp', axis=0, tiled=True)  12.6 us
    all_gather x1, blocking collectives, on_device(): lax.all_gather(query_low, 'tp', axis=0, tiled=True)  9.73 us
    all_gather x1, blocking collectives, on_device(): lax.all_gather(latent_low, 'tp', axis=0, tiled=True)  9.6 us
  transfers between devices with their start and end apart: 3, of which 1 were waited for; matrix products, arithmetic and copies ran while one was open for 2% of the time, Pallas kernels for 0%

profile of v1, /device:TPU:0, one launch (start us, length us, event | category | flops | bytes accessed | tf_op | source)
XLA Modules:
  0.0 152.2 jit_solution(15218846160885765642)
XLA Ops:
  0.0 0.8 fusion.53
  0.9 1.3 fusion.71
  2.1 1.2 fusion.72
  3.4 1.2 fusion.73
  4.6 13.7 %psum.7 = f32[3,512]{1,0:T(4,128)S(1)} all-reduce(f32[3,512]{1,0:T(4,128)S(1)} %pad_maximum_fusion.2), channel_id=1, replica_groups=mesh['sp'=4,'tp'=4,'dp'=2] {'sp'}, use_global_device_ids=true, to_apply=%region_0.1 | all-reduce | flops 1536 | bytes 12288 | tf_op jit(solution)/shard_map/psum | solution.py:102
  18.4 1.5 %collective-permute-start = (f32[3,512]{1,0:T(4,128)S(1)}, f32[3,512]{1,0:T(4,128)S(1)}, u32[]{:S(2)}, u32[]{:S(2)}) collective-permute-start(f32[3,512]{1,0:T(4,128)S(1)} %psum.7), channel_id=1, source_target_pairs={{0,2},{2,4},{4,6},{6,0},{1,3},{3,5},{5,7},{7,1},{8,10},{10,12},{12... | collective-permute-start | bytes 18440 | tf_op jit(solution)/shard_map/ppermute | solution.py:105
  19.9 1.2 fusion.24
  21.1 14.1 %all_gather.25 = bf16[512,256]{1,0:T(8,128)(2,1)S(1)} all-gather(bf16[128,256]{1,0:T(8,128)(2,1)} %param.20), channel_id=1, replica_groups=mesh['sp'=4,'tp'=4,'dp'=2] {'sp'}, dimensions={0}, use_global_device_ids=true | all-gather | bytes 327680 | tf_op jit(solution)/shard_map/all_gather | solution.py:146
  35.8 0.7 broadcast_multiply_fusion.3
  36.6 1.5 %collective-permute-start.1 = (f32[3,512]{1,0:T(4,128)S(1)}, f32[3,512]{1,0:T(4,128)S(1)}, u32[]{:S(2)}, u32[]{:S(2)}) collective-permute-start(f32[3,512]{1,0:T(4,128)S(1)} %collective-permute-done), channel_id=1, source_target_pairs={{0,2},{2,4},{4,6},{6,0},{1,3},{3,5},{5,7},{7,1},{8,10},{10,12},{12... | collective-permute-start | bytes 18440 | tf_op jit(solution)/shard_map/ppermute | solution.py:105
  38.1 0.9 fusion.41
  39.0 2.2 %collective-permute-done.1 = f32[3,512]{1,0:T(4,128)S(1)} collective-permute-done((f32[3,512]{1,0:T(4,128)S(1)}, f32[3,512]{1,0:T(4,128)S(1)}, u32[]{:S(2)}, u32[]{:S(2)}) %collective-permute-start.1) | collective-permute-done | bytes 6176 | tf_op jit(solution)/shard_map/ppermute | solution.py:105
  41.2 0.6 collective-permute-start.2
  41.8 12.6 %all_gather.26 = bf16[512,64]{0,1:T(8,128)(2,1)} all-gather(bf16[128,64]{0,1:T(8,128)(2,1)S(1)} %copy-done.9), channel_id=1, replica_groups=mesh['sp'=4,'tp'=4,'dp'=2] {'sp'}, dimensions={0}, use_global_device_ids=true | all-gather | bytes 81920 | tf_op jit(solution)/shard_map/all_gather | solution.py:147
  54.7 1.7 %multiply_reduce_fusion.1 = (f32[96]{0:T(128)S(1)}, f32[96,256]{1,0:T(8,128)S(1)}) fusion(bf16[2048,256]{1,0:T(8,128)(2,1)} %param.27, bf16[96,2048]{1,0:T(8,128)(2,1)S(1)} %copy-done.1, f32[2048]{0:T(1024)S(1)} %bitcast.122, f32[2048]{0:T(1024)S(1)} %bitcast.119, f32[2048]{0:T(1024)S(1)} %copy-done.16, f32[96]{0:T(128)S(1)} %add_rsqrt_fusion.2), kind=kOutput, calls=%fused_computation.49 | convolution fusion | flops 101892000 | bytes 1565440 | tf_op jit(solution)/shard_map/dot_general | solution.py:120
  56.5 9.6 %all_gather.27 = bf16[384,256]{1,0:T(8,128)(2,1)S(1)} all-gather(bf16[96,256]{1,0:T(8,128)(2,1)S(1)} %multiply_convert_fusion.1), channel_id=1, replica_groups=mesh['sp'=4,'tp'=4,'dp'=2] {'tp'}, dimensions={0}, use_global_device_ids=true | all-gather | bytes 245760 | tf_op jit(solution)/shard_map/all_gather | solution.py:131
  66.5 1.1 fusion.61
  67.7 7.2 %all-gather = bf16[4,96,64]{1,2,0:T(8,128)(2,1)S(1)} all-gather(bf16[1,96,64]{1,2,0:T(8,128)(2,1)S(1)} %fusion.46), channel_id=1, replica_groups=mesh['sp'=4,'tp'=4,'dp'=2] {'tp'}, dimensions={0}, use_global_device_ids=true | all-gather | bytes 61440 | tf_op jit(solution)/shard_map/all_gather | solution.py:132
  75.1 14.1 %all_gather.30 = bf16[1536,64]{0,1:T(8,128)(2,1)S(1)} all-gather(bf16[384,64]{0,1:T(8,128)(2,1)S(1)} %reshape.254), channel_id=1, replica_groups=mesh['sp'=4,'tp'=4,'dp'=2] {'sp'}, dimensions={0}, use_global_device_ids=true | all-gather | bytes 245760 | tf_op jit(solution)/shard_map/all_gather | solution.py:199
  89.3 1.4 multiply_reduce_fusion
  90.8 9.7 %all_gather.24 = bf16[384,512]{1,0:T(8,128)(2,1)S(1)} all-gather(bf16[96,512]{1,0:T(8,128)(2,1)S(1)} %multiply_convert_fusion), channel_id=1, replica_groups=mesh['sp'=4,'tp'=4,'dp'=2] {'tp'}, dimensions={0}, use_global_device_ids=true | all-gather | bytes 491520 | tf_op jit(solution)/shard_map/all_gather | solution.py:130
  101.0 17.7 %all_gather.28 = bf16[1536,256]{1,0:T(8,128)(2,1)S(1)} all-gather(bf16[384,256]{1,0:T(8,128)(2,1)S(1)} %convolution_convert_fusion.3), channel_id=1, replica_groups=mesh['sp'=4,'tp'=4,'dp'=2] {'sp'}, dimensions={0}, use_global_device_ids=true | all-gather | bytes 983040 | tf_op jit(solution)/shard_map/all_gather | solution.py:197
  119.1 0.8 fusion.38
  120.0 1.0 fusion.70
  121.0 0.5 fusion.69
  121.5 0.5 fusion.8
  121.9 15.6 %all_gather.31 = bf16[1536,256]{1,0:T(8,128)(2,1)S(1)} all-gather(bf16[384,256]{1,0:T(8,128)(2,1)S(1)} %convolution_convert_fusion.2), channel_id=1, replica_groups=mesh['sp'=4,'tp'=4,'dp'=2] {'sp'}, dimensions={0}, use_global_device_ids=true | all-gather | bytes 983040 | tf_op jit(solution)/shard_map/all_gather | solution.py:198
  137.5 0.8 fusion.1
  138.4 0.7 fusion.17
  139.1 0.9 fusion.21
  140.3 8.1 %all_to_all.19 = bf16[4,96,256]{2,1,0:T(8,128)(2,1)S(1)} all-to-all(bf16[4,96,256]{2,1,0:T(8,128)(2,1)S(1)} %all_to_all.14), channel_id=1, replica_groups=mesh['sp'=4,'tp'=4,'dp'=2] {'tp'}, dimensions={0} | all-to-all | bytes 393216 | tf_op jit(solution)/shard_map/all_to_all | solution.py:205
  148.4 3.8 %fusion.29 = bf16[96,2048]{1,0:T(8,128)(2,1)} fusion(bf16[96,2048]{1,0:T(8,128)(2,1)S(1)} %copy-done.1, f32[2048]{0:T(1024)S(1)} %bitcast.118, bf16[96,1024]{1,0:T(8,128)(2,1)S(1)} %bitcast.116, bf16[1024,2048]{1,0:T(8,128)(2,1)} %param.35), kind=kOutput, calls=%fused_computation.32 | convolution fusion | flops 403439616 | bytes 5185536 | tf_op jit(solution)/shard_map/dot_general | solution.py:206
  (75 shorter events, 3.0 us)
Async XLA Ops:
  0.0 89.3 %copy-start = (bf16[2048,512]{1,0:T(8,128)(2,1)S(1)}, bf16[2048,512]{1,0:T(8,128)(2,1)}, u32[]{:S(2)}) copy-start(bf16[2048,512]{1,0:T(8,128)(2,1)} %param.26) | copy-start | bytes 6291460
  0.0 54.6 %copy-start.1 = (bf16[96,2048]{1,0:T(8,128)(2,1)S(1)}, bf16[96,2048]{1,0:T(8,128)(2,1)}, u32[]{:S(2)}) copy-start(bf16[96,2048]{1,0:T(8,128)(2,1)} %param.18) | copy-start | bytes 1179652
  0.0 35.3 %copy-start.2 = (bf16[256,256]{1,0:T(8,128)(2,1)S(1)}, bf16[256,256]{1,0:T(8,128)(2,1)}, u32[]{:S(2)}) copy-start(bf16[256,256]{1,0:T(8,128)(2,1)} %param.32) | copy-start | bytes 393220
  0.0 35.5 %copy-start.3 = (bf16[256,256]{1,0:T(8,128)(2,1)S(1)}, bf16[256,256]{1,0:T(8,128)(2,1)}, u32[]{:S(2)}) copy-start(bf16[256,256]{1,0:T(8,128)(2,1)} %param.33) | copy-start | bytes 393220
  0.0 41.8 %copy-start.9 = (bf16[128,64]{0,1:T(8,128)(2,1)S(1)}, bf16[128,64]{0,1:T(8,128)(2,1)}, u32[]{:S(2)}) copy-start(bf16[128,64]{0,1:T(8,128)(2,1)} %param.21) | copy-start | bytes 49156
  0.0 54.6 %copy-start.16 = (f32[2048]{0:T(1024)S(1)}, f32[2048]{0:T(1024)}, u32[]{:S(2)}) copy-start(f32[2048]{0:T(1024)} %param.25) | copy-start | bytes 24580
  4.6 51.8 %copy-start.13 = (f32[256]{0:T(256)S(1)}, f32[256]{0:T(256)}, u32[]{:S(2)}) copy-start(f32[256]{0:T(256)} %param.30) | copy-start | bytes 3076
  18.4 18.2 %collective-permute-start = (f32[3,512]{1,0:T(4,128)S(1)}, f32[3,512]{1,0:T(4,128)S(1)}, u32[]{:S(2)}, u32[]{:S(2)}) collective-permute-start(f32[3,512]{1,0:T(4,128)S(1)} %psum.7), channel_id=1, source_target_pairs={{0,2},{2,4},{4,6},{6,0},{1,3},{3,5},{5,7},{7,1},{8,10},{10,12},{12... | collective-permute-start | bytes 18440 | tf_op jit(solution)/shard_map/ppermute | solution.py:105
  36.6 19.9 %copy-start.17 = (f32[96]{0:T(128)}, f32[96]{0:T(128)S(1)}, u32[]{:S(2)}) copy-start(f32[96]{0:T(128)S(1)} %add_rsqrt_fusion.2) | copy-start | bytes 1156
  36.6 4.6 %collective-permute-start.1 = (f32[3,512]{1,0:T(4,128)S(1)}, f32[3,512]{1,0:T(4,128)S(1)}, u32[]{:S(2)}, u32[]{:S(2)}) collective-permute-start(f32[3,512]{1,0:T(4,128)S(1)} %collective-permute-done), channel_id=1, source_target_pairs={{0,2},{2,4},{4,6},{6,0},{1,3},{3,5},{5,7},{7,1},{8,10},{10,12},{12... | collective-permute-start | bytes 18440 | tf_op jit(solution)/shard_map/ppermute | solution.py:105
  41.2 13.2 %collective-permute-start.2 = (f32[3,512]{1,0:T(4,128)S(1)}, f32[3,512]{1,0:T(4,128)S(1)}, u32[]{:S(2)}, u32[]{:S(2)}) collective-permute-start(f32[3,512]{1,0:T(4,128)S(1)} %collective-permute-done.1), channel_id=1, source_target_pairs={{0,2},{2,4},{4,6},{6,0},{1,3},{3,5},{5,7},{7,1},{8,10},{10,12},{12... | collective-permute-start | bytes 18440 | tf_op jit(solution)/shard_map/ppermute | solution.py:105
  54.4 12.1 %copy-start.15 = (bf16[2048,64]{0,1:T(8,128)(2,1)S(1)}, bf16[2048,64]{0,1:T(8,128)(2,1)}, u32[]{:S(2)}) copy-start(bf16[2048,64]{0,1:T(8,128)(2,1)} %param.28) | copy-start | bytes 786436
  54.6 20.3 %copy-start.10 = (f32[1,2048]{1,0:T(1,128)}, f32[1,2048]{1,0:T(1,128)S(1)}, u32[]{:S(2)}) copy-start(f32[1,2048]{1,0:T(1,128)S(1)} %get-tuple-element.12) | copy-start | bytes 24580
  54.6 20.3 %copy-start.11 = (f32[1,2048]{1,0:T(1,128)}, f32[1,2048]{1,0:T(1,128)S(1)}, u32[]{:S(2)}) copy-start(f32[1,2048]{1,0:T(1,128)S(1)} %get-tuple-element.13) | copy-start | bytes 24580
  54.7 12.9 %copy-start.8 = (f32[96,16]{0,1:T(8,128)S(1)}, f32[96,16]{0,1:T(8,128)}, u32[]{:S(2)}) copy-start(f32[96,16]{0,1:T(8,128)} %get-tuple-element.22) | copy-start | bytes 18436
  66.5 24.1 %copy-start.12 = (f32[512]{0:T(512)S(1)}, f32[512]{0:T(512)}, u32[]{:S(2)}) copy-start(f32[512]{0:T(512)} %param.29) | copy-start | bytes 6148
  75.1 25.4 %copy-start.4 = (bf16[512,384]{1,0:T(8,128)(2,1)S(1)}, bf16[512,384]{1,0:T(8,128)(2,1)}, u32[]{:S(2)}) copy-start(bf16[512,384]{1,0:T(8,128)(2,1)} %param.31) | copy-start | bytes 1179652
  100.5 18.6 %copy-start.5 = (f32[384,64]{0,1:T(8,128)S(1)}, f32[384,64]{0,1:T(8,128)}, u32[]{:S(2)}) copy-start(f32[384,64]{0,1:T(8,128)} %get-tuple-element.14) | copy-start | bytes 294916
  100.5 18.6 %copy-start.6 = (f32[384,64]{0,1:T(8,128)S(1)}, f32[384,64]{0,1:T(8,128)}, u32[]{:S(2)}) copy-start(f32[384,64]{0,1:T(8,128)} %get-tuple-element.15) | copy-start | bytes 294916
  119.9 1.0 copy-start.7
  120.0 1.0 copy-start.14
